TPU v7x, 32 devices: a whole 2x2x4 slice. The times are simulated.
32 devices in a mesh: tp: 8 (over z, y), dp: 4 (over x, core).
Axes of the slice: x: 2, y: 2, z: 4, core: 2. Of those that a mesh axis runs over, the one named last changes fastest.
Arguments:
- tokens: bfloat16 [128, 4096], P('tp', 'dp'), may hold values from -10 to 10
- norm_gain: float32 [2, 4096], P(None, 'dp'), may hold values from 0.1 to 1.9
- input_weight: bfloat16 [2, 4096, 1024], P(None, 'dp', 'tp'), may hold values from -0.09375 to 0.09375
- decay_rate: float32 [2, 64, 64], P(None, 'tp'), may hold values from 0.01 to 1
- frequency: float32 [2, 64, 64], P(None, 'tp'), may hold values from 0.5 to 3
- step_size: float32 [2, 64], P(None, 'tp'), may hold values from 0.1 to 1
- state_in: float32 [2, 64, 16, 128], P(None, 'tp'), may hold values from -1.5 to 1.5
- readout: float32 [2, 64, 16, 128], P(None, 'tp'), may hold values from -0.5 to 0.5
- skip_gain: float32 [2, 1024], P(None, 'tp'), may hold values from -3 to 3
- value_weight: bfloat16 [2, 1024, 4096], P(None, 'tp', 'dp'), may hold values from -0.1875 to 0.1875
- gate_weight: bfloat16 [2, 1024, 4096], P(None, 'tp', 'dp'), may hold values from -0.1875 to 0.1875
- states: float32 [2, 128, 64, 128], P(None, 'dp', 'tp'), may hold values from -3 to 3
Outputs:
- tokens_out: bfloat16 [128, 4096], P('tp', 'dp')
- states_out: float32 [2, 128, 64, 128], P(None, 'dp', 'tp')
All inputs are finite; a program needn't handle non-finite values.
Results may differ from a plain program's by a relative error of at most 0.007.
Values may be sent and summed in bfloat16 or wider, within the bound.
A program may use at most 64 MiB of HBM per device.

v0:
```python
import jax
import jax.numpy as jnp
from jax import lax
from jax.sharding import PartitionSpec as P

D = 4096
LAYERS = 2


epsilon = 1e-06


def transition(rate, frequency, step):
    magnitude = jnp.exp(-rate * step[:, None])
    angle = frequency * step[:, None]
    keep_real = magnitude * jnp.cos(angle)
    keep_imag = magnitude * jnp.sin(angle)
    minus_one = keep_real - 1.0
    denominator = rate * rate + frequency * frequency
    lift_real = (-minus_one * rate + keep_imag * frequency) / denominator
    lift_imag = (-keep_imag * rate - minus_one * frequency) / denominator
    return (keep_real, keep_imag, lift_real, lift_imag)


def update(drive, state, rate, frequency, step, state_in, readout, skip):
    groups = rate.shape[0]
    half = state.shape[-1] // 2
    grouped = drive.reshape(drive.shape[0], groups, -1)
    pushed = jnp.einsum("sgc,gcq->sgq", grouped, state_in, precision=lax.Precision.HIGHEST)
    keep_real, keep_imag, lift_real, lift_imag = transition(rate, frequency, step)
    push_real, push_imag = (pushed[..., :half], pushed[..., half:])
    old_real, old_imag = (state[..., :half], state[..., half:])
    new_real = (
        keep_real * old_real - keep_imag * old_imag + lift_real * push_real - lift_imag * push_imag
    )
    new_imag = (
        keep_real * old_imag + keep_imag * old_real + lift_real * push_imag + lift_imag * push_real
    )
    new_state = jnp.concatenate([new_real, new_imag], axis=-1)
    summed = jnp.einsum("sgq,gcq->sgc", new_state, readout, precision=lax.Precision.HIGHEST)
    value = summed.reshape(drive.shape) + skip[None, :] * drive
    return (new_state, jax.nn.gelu(value).astype(jnp.bfloat16))


def body(
    tokens,
    norm_gain,
    input_weight,
    decay_rate,
    frequency,
    step_size,
    state_in,
    readout,
    skip_gain,
    value_weight,
    gate_weight,
    states,
):
    current = tokens
    own_rows = states.shape[1]
    offset = lax.axis_index("dp") * own_rows
    width_dev = tokens.shape[1]
    updated = []
    for depth_index in range(LAYERS):
        whole = lax.all_gather(current, "tp", axis=0, tiled=True)
        widened = whole.astype(jnp.float32)
        squares = jnp.sum(widened * widened, axis=1)
        gained = (widened * norm_gain[depth_index][None, :]).astype(jnp.bfloat16)
        weight_in = input_weight[depth_index]
        totals = lax.psum(squares, "dp")
        own_squares = lax.dynamic_slice_in_dim(totals, offset, own_rows)
        summed = lax.psum_scatter(
            jnp.dot(gained, weight_in, preferred_element_type=jnp.float32),
            "dp",
            scatter_dimension=0,
            tiled=True,
        )
        drive = summed * lax.rsqrt(own_squares / D + epsilon)[:, None]
        new_state, readout_value = update(
            drive,
            states[depth_index],
            decay_rate[depth_index],
            frequency[depth_index],
            step_size[depth_index],
            state_in[depth_index],
            readout[depth_index],
            skip_gain[depth_index],
        )
        updated.append(new_state)
        ready = lax.all_gather(readout_value, "dp", axis=0, tiled=True)
        value_rows = value_weight[depth_index]
        gate_rows = gate_weight[depth_index]
        both = lax.psum_scatter(
            jnp.concatenate(
                [
                    jnp.dot(ready, value_rows, preferred_element_type=jnp.float32),
                    jnp.dot(ready, gate_rows, preferred_element_type=jnp.float32),
                ],
                axis=1,
            ),
            "tp",
            scatter_dimension=0,
            tiled=True,
        )
        value, gate = (both[:, :width_dev], both[:, width_dev:])
        current = (current.astype(jnp.float32) + value * jax.nn.sigmoid(gate)).astype(jnp.bfloat16)
    return (current, jnp.stack(updated))


def solution(mesh):
    in_specs = (
        P("tp", "dp"),
        P(None, "dp"),
        P(None, "dp", "tp"),
        P(None, "tp", None),
        P(None, "tp", None),
        P(None, "tp"),
        P(None, "tp", None, None),
        P(None, "tp", None, None),
        P(None, "tp"),
        P(None, "tp", "dp"),
        P(None, "tp", "dp"),
        P(None, "dp", "tp", None),
    )
    out_specs = (P("tp", "dp"), P(None, "dp", "tp", None))
    return jax.shard_map(body, mesh=mesh, in_specs=in_specs, out_specs=out_specs, check_vma=False)
```

profile of v0, /device:TPU:0, one launch (start us, length us, event | category | flops | bytes accessed | tf_op | source)
XLA Modules:
  0.0 270.4 jit_solution(15485128415687994219)
XLA Ops:
  7.2 0.8 fusion.73
  8.0 32.8 %all_gather.12 = bf16[128,1024]{1,0:T(8,128)(2,1)S(1)} all-gather(bf16[16,1024]{1,0:T(8,128)(2,1)} %param.12), channel_id=1, replica_groups=mesh['tp'=8,'dp'=4] {'tp'}, dimensions={0}, use_global_device_ids=true | all-gather | bytes 294912 | tf_op jit(solution)/shard_map/all_gather | solution.py:65
  40.8 1.8 fusion.6
  42.7 0.6 copy-done.10
  43.4 0.6 copy-done.8
  44.1 0.1 fusion.66
  44.2 0.1 fusion.1
  44.3 5.8 %psum.14 = f32[128]{0:T(128)S(1)} all-reduce(f32[128]{0:T(128)S(1)} %fusion.1), channel_id=1, replica_groups=mesh['tp'=8,'dp'=4] {'dp'}, use_global_device_ids=true, to_apply=%region_2.0 | all-reduce | flops 128 | bytes 1024 | tf_op jit(solution)/shard_map/psum | solution.py:70
  50.1 0.1 add_rsqrt_fusion.1
  50.2 13.1 %reduce-scatter.5.cloned.1.call-done = f32[32,128]{1,0:T(8,128)} async-done(((f32[128,128]{1,0:T(8,128)}), f32[32,128]{1,0:T(8,128)}) %reduce-scatter.5.cloned.1.call-update) | async-done | bytes 16400 | tf_op jit(solution)/shard_map/reduce_scatter | solution.py:72
  63.4 0.8 broadcast_multiply_fusion.1
  64.1 0.1 copy.22
  64.2 0.4 convolution_bitcast_fusion.1
  64.7 0.1 multiply_subtract_fusion.1
  64.8 0.7 copy-done.5
  65.6 0.4 fusion.39
  66.0 0.1 copy.23
  66.0 0.2 copy-done.6
  66.3 0.1 fusion.57
  66.4 5.2 %all_gather.13 = bf16[128,128]{1,0:T(8,128)(2,1)S(1)} all-gather(bf16[32,128]{1,0:T(8,128)(2,1)S(1)} %fusion.57), channel_id=1, replica_groups=mesh['tp'=8,'dp'=4] {'dp'}, dimensions={0}, use_global_device_ids=true | all-gather | bytes 40960 | tf_op jit(solution)/shard_map/all_gather | solution.py:90
  71.6 0.2 fusion.13
  71.8 0.2 fusion.15
  72.0 1.0 pad_maximum_fusion
  73.1 64.3 %reduce-scatter.7.cloned.1.call-done = f32[16,2048]{1,0:T(8,128)} async-done(((f32[128,2048]{1,0:T(8,128)}), f32[16,2048]{1,0:T(8,128)}) %reduce-scatter.7.cloned.1.call-update) | async-done | bytes 131088 | tf_op jit(solution)/shard_map/reduce_scatter | solution.py:93
  137.4 0.9 fusion.46
  138.3 30.8 %all_gather.14 = bf16[128,1024]{1,0:T(8,128)(2,1)S(1)} all-gather(bf16[16,1024]{1,0:T(8,128)(2,1)S(1)} %fusion.46), channel_id=1, replica_groups=mesh['tp'=8,'dp'=4] {'tp'}, dimensions={0}, use_global_device_ids=true | all-gather | bytes 294912 | tf_op jit(solution)/shard_map/all_gather | solution.py:65
  169.2 0.9 fusion.4
  170.1 0.1 fusion.3
  170.3 5.7 %psum.15 = f32[128]{0:T(128)S(1)} all-reduce(f32[128]{0:T(128)S(1)} %fusion.3), channel_id=1, replica_groups=mesh['tp'=8,'dp'=4] {'dp'}, use_global_device_ids=true, to_apply=%region_6.0 | all-reduce | flops 128 | bytes 1024 | tf_op jit(solution)/shard_map/psum | solution.py:70
  175.9 0.1 add_rsqrt_fusion
  176.0 12.6 %reduce-scatter.9.cloned.1.call-done = f32[32,128]{1,0:T(8,128)} async-done(((f32[128,128]{1,0:T(8,128)}), f32[32,128]{1,0:T(8,128)}) %reduce-scatter.9.cloned.1.call-update) | async-done | bytes 16400 | tf_op jit(solution)/shard_map/reduce_scatter | solution.py:72
  188.6 0.8 broadcast_multiply_fusion
  189.4 0.1 copy.25
  189.5 0.4 convolution_bitcast_fusion
  190.0 0.1 multiply_subtract_fusion
  190.1 0.4 fusion.36
  190.5 0.1 copy.26
  190.6 0.7 copy-done.7
  191.2 0.1 fusion.65
  191.3 5.2 %all_gather.15 = bf16[128,128]{1,0:T(8,128)(2,1)S(1)} all-gather(bf16[32,128]{1,0:T(8,128)(2,1)S(1)} %fusion.65), channel_id=1, replica_groups=mesh['tp'=8,'dp'=4] {'dp'}, dimensions={0}, use_global_device_ids=true | all-gather | bytes 40960 | tf_op jit(solution)/shard_map/all_gather | solution.py:90
  196.5 0.2 fusion.8
  196.7 0.2 fusion.10
  196.9 1.0 pad_maximum_fusion.1
  198.0 0.1 fusion.49
  198.1 0.1 fusion.48
  198.2 0.9 copy.27
  199.1 63.2 %reduce-scatter.11.cloned.1.call-done = f32[16,2048]{1,0:T(8,128)} async-done(((f32[128,2048]{1,0:T(8,128)}), f32[16,2048]{1,0:T(8,128)}) %reduce-scatter.11.cloned.1.call-update) | async-done | bytes 131088 | tf_op jit(solution)/shard_map/reduce_scatter | solution.py:93
  262.4 1.5 fusion.47
  (34 shorter events, 0.4 us)
Async XLA Ops:
  7.2 56.2 %reduce-scatter.5.cloned.1.call-start = ((), (), s32[]{:S(2)}) async-start(), calls=%async_computation.4 | async-start | bytes 81920 | tf_op jit(solution)/shard_map/reduce_scatter | solution.py:72
  40.8 2.6 copy-start.2
  42.6 0.7 copy-start.10
  42.6 0.7 copy-start.11
  42.7 94.8 %reduce-scatter.7.cloned.1.call-start = ((), (), s32[]{:S(2)}) async-start(), calls=%async_computation.5 | async-start | bytes 1179648 | tf_op jit(solution)/shard_map/reduce_scatter | solution.py:93
  43.4 0.7 copy-start.8
  43.4 0.7 copy-start.9
  44.3 19.9 %copy-start.4 = (f32[2,8,16,128]{3,2,1,0:T(8,128)S(1)}, f32[2,8,16,128]{3,2,1,0:T(8,128)}, u32[]{:S(2)}) copy-start(f32[2,8,16,128]{3,2,1,0:T(8,128)} %param.18) | copy-start | bytes 393220
  64.7 0.9 copy-start.5
  64.7 6.9 %copy-start = (bf16[2,128,1024]{2,1,0:T(8,128)(2,1)S(1)}, bf16[2,128,1024]{2,1,0:T(8,128)(2,1)}, u32[]{:S(2)}) copy-start(bf16[2,128,1024]{2,1,0:T(8,128)(2,1)} %param.22) | copy-start | bytes 1572868
  65.6 0.7 copy-start.6
  66.0 5.8 %copy-start.1 = (bf16[2,128,1024]{2,1,0:T(8,128)(2,1)S(1)}, bf16[2,128,1024]{2,1,0:T(8,128)(2,1)}, u32[]{:S(2)}) copy-start(bf16[2,128,1024]{2,1,0:T(8,128)(2,1)} %param.21) | copy-start | bytes 1572868
  73.1 64.4 %copy-start.3 = (bf16[16,1024]{1,0:T(8,128)(2,1)S(1)}, bf16[16,1024]{1,0:T(8,128)(2,1)}, u32[]{:S(2)}) copy-start(bf16[16,1024]{1,0:T(8,128)(2,1)} %param.12) | copy-start | bytes 98308
  73.1 96.1 %copy-start.12 = (bf16[2,1024,128]{2,1,0:T(8,128)(2,1)S(1)}, bf16[2,1024,128]{2,1,0:T(8,128)(2,1)}, u32[]{:S(2)}) copy-start(bf16[2,1024,128]{2,1,0:T(8,128)(2,1)} %param.14) | copy-start | bytes 1572868
  73.1 115.5 %reduce-scatter.9.cloned.1.call-start = ((), (), s32[]{:S(2)}) async-start(), calls=%async_computation.6 | async-start | bytes 81920 | tf_op jit(solution)/shard_map/reduce_scatter | solution.py:72
  170.1 92.3 %reduce-scatter.11.cloned.1.call-start = ((), (), s32[]{:S(2)}) async-start(), calls=%async_computation.7 | async-start | bytes 1179648 | tf_op jit(solution)/shard_map/reduce_scatter | solution.py:93
  190.5 0.7 copy-start.7
Sparse Core Ops, SparseCore 0:
  42.8 20.5 reduce-scatter.4
  73.2 64.1 reduce-scatter.6
  170.2 18.3 reduce-scatter.8
  198.1 64.1 reduce-scatter.10
where the time goes:
time: 271 us; the launch traced here: 270 us
  waiting for transfers between devices  153 us (56%)
  blocking collectives  85.4 us (32%)
  between operations  14 us (5%)
  other arithmetic  7.3 us (3%)
  matrix products  5.18 us (2%)
  local copies, waits for them, and re-layouts  4.96 us (2%)
    reduce_scatter x2, waiting for transfers between devices, body(): lax.psum_scatter(jnp.concatenate([jnp.dot(ready, value_rows, preferred_el...  128 us
    all_gather x2, blocking collectives, body(): whole = lax.all_gather(current, 'tp', axis=0, tiled=True)  63.6 us
    reduce_scatter x2, waiting for transfers between devices, body(): lax.psum_scatter(jnp.dot(gained, weight_in, preferred_element_type=jnp.fl...  25.8 us
    psum x2, blocking collectives, body(): totals = lax.psum(squares, 'dp')  11.5 us
    all_gather x2, blocking collectives, body(): ready = lax.all_gather(readout_value, 'dp', axis=0, tiled=True)  10.4 us
  transfers between devices with their start and end apart: 4, of which 4 were waited for; matrix products, arithmetic and copies ran while one was open for 1% of the time, Pallas kernels for 0%

commit v1 on v0

v1 whole, which is shorter than its diff:
```python
import functools

import jax
import jax.numpy as jnp
from jax import lax
from jax.experimental import pallas as pl
from jax.experimental.pallas import tpu as pltpu
from jax.sharding import PartitionSpec as P

epsilon = 1e-06
HIGHEST = lax.Precision.HIGHEST
NT = (((1,), (1,)), ((), ()))


def iota(shape, axis):
    return lax.broadcasted_iota(jnp.int32, shape, axis)


def kernel(n_tp, n_dp, width, *refs):
    ins, refs = refs[:12], refs[12:]
    (out_tok, out_st), refs = refs[:2], refs[2:]
    held, refs = refs[:11], refs[11:]
    (gain_v, win_v, rate_v, freq_v, step_v, sin_v, rout_v, skip_v, vw_v, gw_v, st_v) = held
    (xg, sq_s, sq_r, part_s, part_r, ready, prod_s, prod_r, keep_v, base_v, lift_v, mix_v, new_v,
     load_sem, out_sem, x_sem, sq_sem, part_sem, ready_sem, prod_sem) = refs
    layers, rows, groups, entries = st_v.shape
    chans = part_s.shape[-1]
    per = chans // groups
    batch = n_dp * rows
    local = xg.shape[-1]
    t = lax.axis_index("tp")
    d = lax.axis_index("dp")

    loads = [pltpu.make_async_copy(ins[0], xg.at[0, t], load_sem.at[0])]
    for i in range(11):
        loads.append(pltpu.make_async_copy(ins[i + 1], held[i], load_sem.at[i + 1]))
    for i in (0, 3, 4, 5, 6, 7, 11, 8, 1, 2, 9, 10):
        loads[i].start()

    barrier = pltpu.get_barrier_semaphore()
    for k in range(1, n_tp):
        pl.semaphore_signal(barrier, inc=1, device_id={"tp": lax.rem(t + k, n_tp)},
                            device_id_type=pl.DeviceIdType.MESH)
    for k in range(1, n_dp):
        pl.semaphore_signal(barrier, inc=1, device_id={"dp": lax.rem(d + k, n_dp)},
                            device_id_type=pl.DeviceIdType.MESH)

    pending = []

    def send(axis, k, src, dst, sems, index):
        me, n = (t, n_tp) if axis == "tp" else (d, n_dp)
        copy = pltpu.make_async_remote_copy(
            src_ref=src, dst_ref=dst,
            send_sem=sems.at[(0,) + index], recv_sem=sems.at[(1,) + index],
            device_id={axis: lax.rem(me + k, n)}, device_id_type=pl.DeviceIdType.MESH)
        copy.start()
        pending.append(copy)
        return copy

    def send_tokens(layer):
        return [send("tp", k, xg.at[layer, t], xg.at[layer, t], x_sem, (layer, k))
                for k in range(1, n_tp)]

    def prepare(layer):
        half = entries // 2
        diagonal = iota((groups, groups), 0) == iota((groups, groups), 1)
        step = jnp.sum(jnp.where(diagonal, step_v[layer][None, :], 0.0), axis=1, keepdims=True)
        rate = jnp.concatenate([rate_v[layer]] * 2, axis=1)
        freq = jnp.concatenate([freq_v[layer]] * 2, axis=1)
        sign = jnp.where(iota((groups, entries), 1) < half, -1.0, 1.0)
        magnitude = jnp.exp(-rate * step)
        angle = freq * step
        keep_real = magnitude * jnp.cos(angle)
        keep_imag = magnitude * jnp.sin(angle)
        minus_one = keep_real - 1.0
        denominator = rate * rate + freq * freq
        lift_real = (-minus_one * rate + keep_imag * freq) / denominator
        lift_imag = sign * (-keep_imag * rate - minus_one * freq) / denominator
        keep_imag = sign * keep_imag

        def swap(value):
            return jnp.concatenate([value[..., half:], value[..., :half]], axis=-1)

        matrix = sin_v[layer]
        lifted = lift_real[:, None, :] * matrix + lift_imag[:, None, :] * swap(matrix)
        lifted = lifted.reshape(chans, entries)
        read = rout_v[layer].reshape(chans, entries)
        mixed = lax.dot_general(lifted, read, NT, precision=HIGHEST,
                                preferred_element_type=jnp.float32)
        first, second = iota((chans, chans), 0), iota((chans, chans), 1)
        mixed = jnp.where(first // per == second // per, mixed, 0.0)
        mixed = mixed + jnp.where(first == second, skip_v[layer][None, :], 0.0)
        old = st_v[layer]
        kept = keep_real[None] * old + keep_imag[None] * swap(old)
        base = lax.dot_general(kept.reshape(rows * groups, entries), read, NT, precision=HIGHEST,
                               preferred_element_type=jnp.float32).reshape(rows, groups, chans)
        own = iota((groups, chans), 0) == iota((groups, chans), 1) // per
        keep_v[layer] = kept
        base_v[layer] = jnp.sum(jnp.where(own[None], base, 0.0), axis=1)
        lift_v[layer] = lifted
        mix_v[layer] = mixed

    loads[0].wait()
    pl.semaphore_wait(barrier, n_tp + n_dp - 2)
    sent = send_tokens(0)
    for i in (3, 4, 5, 6, 7, 11, 8):
        loads[i].wait()
    prepare(0)
    for i in (1, 2, 9, 10):
        loads[i].wait()
    outs = []

    for layer in range(layers):
        for copy in sent:
            copy.wait_recv()
        x = xg[layer].reshape(batch, local).astype(jnp.float32)
        square = jnp.sum(x * x, axis=1, keepdims=True)
        eye = iota((batch, batch), 0) == iota((batch, batch), 1)
        line = jnp.sum(jnp.where(eye, square, 0.0), axis=0, keepdims=True)
        sq_s[layer] = jnp.broadcast_to(line, (8, batch))
        sent = [send("dp", k, sq_s.at[layer], sq_r.at[layer, d], sq_sem, (layer, k))
                for k in range(1, n_dp)]
        gained = (x * gain_v[layer][None, :]).astype(jnp.bfloat16)
        part = jnp.dot(gained, win_v[layer], preferred_element_type=jnp.float32)
        part_s[layer] = part.reshape(n_dp, rows, chans)
        for k in range(1, n_dp):
            sent.append(send("dp", k, part_s.at[layer, lax.rem(d + k, n_dp)],
                             part_r.at[layer, d], part_sem, (layer, k)))
        total = part_s[layer, d]
        for copy in sent:
            copy.wait_recv()
        for k in range(1, n_dp):
            source = lax.rem(d + n_dp - k, n_dp)
            total += part_r[layer, source]
            line += sq_r[layer, source][:1]
        pick = iota((rows, batch), 1) == iota((rows, batch), 0) + d * rows
        square = jnp.sum(jnp.where(pick, line, 0.0), axis=1, keepdims=True)
        drive = total * lax.rsqrt(square / width + epsilon)
        value = base_v[layer] + jnp.dot(drive, mix_v[layer], precision=HIGHEST,
                                        preferred_element_type=jnp.float32)
        ready[layer, d] = jax.nn.gelu(value).astype(jnp.bfloat16)
        sent = [send("dp", k, ready.at[layer, d], ready.at[layer, d], ready_sem, (layer, k))
                for k in range(1, n_dp)]
        own = iota((groups, chans), 0) == iota((groups, chans), 1) // per
        spread = jnp.where(own[None], drive[:, None, :], 0.0).reshape(rows * groups, chans)
        push = jnp.dot(spread, lift_v[layer], precision=HIGHEST, preferred_element_type=jnp.float32)
        new_v[layer] = keep_v[layer] + push.reshape(rows, groups, entries)
        out = pltpu.make_async_copy(new_v.at[layer], out_st.at[layer], out_sem.at[layer])
        out.start()
        outs.append(out)
        for copy in sent:
            copy.wait_recv()
        every = ready[layer].reshape(batch, chans)
        for half, weight in ((0, vw_v), (1, gw_v)):
            product = jnp.dot(every, weight[layer], preferred_element_type=jnp.float32)
            prod_s[layer, half] = product.astype(jnp.bfloat16).reshape(n_tp, batch // n_tp, local)
        sent = []
        for half in range(2):
            for k in range(1, n_tp):
                sent.append(send("tp", k, prod_s.at[layer, half, lax.rem(t + k, n_tp)],
                                 prod_r.at[layer, half, t], prod_sem, (layer, half, k)))
        if layer + 1 < layers:
            prepare(layer + 1)
        for copy in sent:
            copy.wait_recv()
        both = []
        for half in range(2):
            total = prod_s[layer, half, t].astype(jnp.float32)
            for k in range(1, n_tp):
                total += prod_r[layer, half, lax.rem(t + n_tp - k, n_tp)].astype(jnp.float32)
            both.append(total)
        current = xg[layer, t].astype(jnp.float32) + both[0] * jax.nn.sigmoid(both[1])
        if layer + 1 < layers:
            xg[layer + 1, t] = current.astype(jnp.bfloat16)
            sent = send_tokens(layer + 1)
        else:
            out_tok[...] = current.astype(jnp.bfloat16)
    for out in outs:
        out.wait()
    for copy in pending:
        copy.wait_send()


def body(n_tp, n_dp, *args):
    tokens, states, win = args[0], args[11], args[2]
    layers, rows, groups, entries = states.shape
    local, chans = tokens.shape[1], win.shape[2]
    own, batch = tokens.shape[0], rows * n_dp
    f32, bf16 = jnp.float32, jnp.bfloat16
    dma = pltpu.SemaphoreType.DMA
    any_spec = pl.BlockSpec(memory_space=pl.ANY)
    scratch = [pltpu.VMEM(a.shape, a.dtype) for a in args[1:]]
    scratch += [
        pltpu.VMEM((layers, n_tp, own, local), bf16),
        pltpu.VMEM((layers, 8, batch), f32),
        pltpu.VMEM((layers, n_dp, 8, batch), f32),
        pltpu.VMEM((layers, n_dp, rows, chans), f32),
        pltpu.VMEM((layers, n_dp, rows, chans), f32),
        pltpu.VMEM((layers, n_dp, rows, chans), bf16),
        pltpu.VMEM((layers, 2, n_tp, own, local), bf16),
        pltpu.VMEM((layers, 2, n_tp, own, local), bf16),
        pltpu.VMEM((layers, rows, groups, entries), f32),
        pltpu.VMEM((layers, rows, chans), f32),
        pltpu.VMEM((layers, chans, entries), f32),
        pltpu.VMEM((layers, chans, chans), f32),
        pltpu.VMEM((layers, rows, groups, entries), f32),
        dma((12,)), dma((layers,)), dma((2, layers, n_tp)), dma((2, layers, n_dp)),
        dma((2, layers, n_dp)), dma((2, layers, n_dp)), dma((2, layers, 2, n_tp)),
    ]
    return pl.pallas_call(
        functools.partial(kernel, n_tp, n_dp, float(local * n_dp)),
        out_shape=(jax.ShapeDtypeStruct(tokens.shape, bf16),
                   jax.ShapeDtypeStruct(states.shape, f32)),
        in_specs=[any_spec] * 12,
        out_specs=(pl.BlockSpec(memory_space=pltpu.VMEM), any_spec),
        scratch_shapes=scratch,
        compiler_params=pltpu.CompilerParams(
            collective_id=0, has_side_effects=True, vmem_limit_bytes=48 * 2**20),
    )(*args)


def solution(mesh):
    in_specs = (
        P("tp", "dp"),
        P(None, "dp"),
        P(None, "dp", "tp"),
        P(None, "tp", None),
        P(None, "tp", None),
        P(None, "tp"),
        P(None, "tp", None, None),
        P(None, "tp", None, None),
        P(None, "tp"),
        P(None, "tp", "dp"),
        P(None, "tp", "dp"),
        P(None, "dp", "tp", None),
    )
    out_specs = (P("tp", "dp"), P(None, "dp", "tp", None))
    run = functools.partial(body, mesh.shape["tp"], mesh.shape["dp"])
    return jax.shard_map(run, mesh=mesh, in_specs=in_specs, out_specs=out_specs, check_vma=False)
```

time: 271 us -> 72.5 us (0.27)
  waiting for transfers between devices: 153 us -> 0 us
  blocking collectives: 85.4 us -> 0 us
  Pallas kernels: 0 us -> 59.8 us
  between operations: 14 us -> 0.66 us
  other arithmetic: 7.3 us -> 0 us
  local copies, waits for them, and re-layouts: 4.96 us -> 11.4 us
  matrix products: 5.18 us -> 0 us
    reduce_scatter x4 -> x0, waiting for transfers between devices: 153 us -> none  [the longest x2 128 us: body(): lax.psum_scatter(jnp.concatenate([jnp.dot(ready, value_rows, preferred_el...]
    all_gather x4 -> x0, blocking collectives: 74 us -> none  [the longest x2 63.6 us: body(): whole = lax.all_gather(current, 'tp', axis=0, tiled=True)]
    pallas_call x0 -> x1, Pallas kernels: none -> 59.8 us  [body(): pl.pallas_call(functools.partial(kernel, n_tp, n_dp, float(local * n_dp))...]
    psum x2 -> x0, blocking collectives: 11.5 us -> none  [body(): totals = lax.psum(squares, 'dp')]
    unnamed x27 -> x26, local copies, waits for them, and re-layouts: 3.79 us -> 11.4 us
    dot_general x10 -> x0, matrix products: 5.18 us -> none  [the longest x2 2.71 us: body(): jnp.dot(gained, weight_in, preferred_element_type=jnp.float32)]
  transfers between devices with their start and end apart: 4 -> 0, of which waited for: 4 -> 0; matrix products, arithmetic and copies ran while one was open for 1% -> 0% of each run, Pallas kernels for 0% -> 0%
where the time goes in v1:
time: 72.5 us; the launch traced here: 71.9 us
  Pallas kernels  59.8 us (82%)
  local copies, waits for them, and re-layouts  11.4 us (16%)
    pallas_call x1, Pallas kernels, body(): pl.pallas_call(functools.partial(kernel, n_tp, n_dp, float(local * n_dp))...  59.8 us
    unnamed x26, local copies, waits for them, and re-layouts  11.4 us

profile of v1, /device:TPU:0, one launch (start us, length us, event | category | flops | bytes accessed | tf_op | source)
XLA Modules:
  0.0 71.9 jit_solution(3694433139869955683)
XLA Ops:
  0.6 0.0 copy-start
  0.6 1.0 %copy-done = bf16[2,1024,128]{2,1,0:T(8,128)(2,1)S(1)} copy-done((bf16[2,1024,128]{2,1,0:T(8,128)(2,1)S(1)}, bf16[2,1024,128]{2,1,0:T(8,128)(2,1)}, u32[]{:S(2)}) %copy-start) | copy-done | bytes 524312
  1.7 0.0 copy-start.1
  1.7 1.0 %copy-done.1 = bf16[2,128,1024]{2,1,0:T(8,128)(2,1)S(1)} copy-done((bf16[2,128,1024]{2,1,0:T(8,128)(2,1)S(1)}, bf16[2,128,1024]{2,1,0:T(8,128)(2,1)}, u32[]{:S(2)}) %copy-start.1) | copy-done | bytes 524312
  2.7 0.0 copy-start.2
  2.7 1.0 %copy-done.2 = bf16[2,128,1024]{2,1,0:T(8,128)(2,1)S(1)} copy-done((bf16[2,128,1024]{2,1,0:T(8,128)(2,1)S(1)}, bf16[2,128,1024]{2,1,0:T(8,128)(2,1)}, u32[]{:S(2)}) %copy-start.2) | copy-done | bytes 524312
  3.8 0.0 copy-start.3
  3.8 0.9 %copy-done.3 = f32[2,32,8,128]{3,2,1,0:T(8,128)S(1)} copy-done((f32[2,32,8,128]{3,2,1,0:T(8,128)S(1)}, f32[2,32,8,128]{3,2,1,0:T(8,128)}, u32[]{:S(2)}) %copy-start.3) | copy-done | bytes 262168
  4.7 0.0 copy-start.4
  4.7 0.9 %copy-done.4 = f32[2,8,16,128]{3,2,1,0:T(8,128)S(1)} copy-done((f32[2,8,16,128]{3,2,1,0:T(8,128)S(1)}, f32[2,8,16,128]{3,2,1,0:T(8,128)}, u32[]{:S(2)}) %copy-start.4) | copy-done | bytes 131096
  5.6 0.0 copy-start.5
  5.6 0.9 %copy-done.5 = f32[2,8,16,128]{3,2,1,0:T(8,128)S(1)} copy-done((f32[2,8,16,128]{3,2,1,0:T(8,128)S(1)}, f32[2,8,16,128]{3,2,1,0:T(8,128)}, u32[]{:S(2)}) %copy-start.5) | copy-done | bytes 131096
  6.5 0.0 copy-start.6
  6.5 0.8 %copy-done.6 = bf16[16,1024]{1,0:T(8,128)(2,1)S(1)} copy-done((bf16[16,1024]{1,0:T(8,128)(2,1)S(1)}, bf16[16,1024]{1,0:T(8,128)(2,1)}, u32[]{:S(2)}) %copy-start.6) | copy-done | bytes 32792
  7.3 0.0 copy-start.7
  7.3 0.7 copy-done.7
  8.0 0.0 copy-start.8
  8.0 0.7 copy-done.8
  8.7 0.0 copy-start.9
  8.7 0.7 copy-done.9
  9.4 0.0 copy-start.10
  9.4 0.7 copy-done.10
  10.1 0.0 copy-start.11
  10.1 0.7 copy-done.11
  10.7 59.8 %shard_map.131 = (bf16[16,1024]{1,0:T(8,128)(2,1)S(1)}, f32[2,32,8,128]{3,2,1,0:T(8,128)S(1)}) custom-call(bf16[16,1024]{1,0:T(8,128)(2,1)S(1)} %copy-done.6, f32[2,1024]{1,0:T(2,128)S(1)} %copy-done.7, bf16[2,1024,128]{2,1,0:T(8,128)(2,1)S(1)} %copy-done, f32[2,8,64]{2,1,0:T(8,128)S(1)} %copy-done.8, f32[2,8,64]{2,1,0:T(8,128)S(1)} %copy-done.9, ...), custom_call_target="tpu_custom_call" | custom-call | tf_op jit(solution)/shard_map/pallas_call | solution.py:210
  70.6 0.6 copy.16
  71.2 0.7 copy.17
Async XLA Ops:
  0.6 1.0 %copy-start = (bf16[2,1024,128]{2,1,0:T(8,128)(2,1)S(1)}, bf16[2,1024,128]{2,1,0:T(8,128)(2,1)}, u32[]{:S(2)}) copy-start(bf16[2,1024,128]{2,1,0:T(8,128)(2,1)} %refs_2_.1) | copy-start | bytes 1572868
  1.7 1.0 %copy-start.1 = (bf16[2,128,1024]{2,1,0:T(8,128)(2,1)S(1)}, bf16[2,128,1024]{2,1,0:T(8,128)(2,1)}, u32[]{:S(2)}) copy-start(bf16[2,128,1024]{2,1,0:T(8,128)(2,1)} %refs_9_.1) | copy-start | bytes 1572868
  2.7 1.0 %copy-start.2 = (bf16[2,128,1024]{2,1,0:T(8,128)(2,1)S(1)}, bf16[2,128,1024]{2,1,0:T(8,128)(2,1)}, u32[]{:S(2)}) copy-start(bf16[2,128,1024]{2,1,0:T(8,128)(2,1)} %refs_10_.1) | copy-start | bytes 1572868
  3.8 0.9 %copy-start.3 = (f32[2,32,8,128]{3,2,1,0:T(8,128)S(1)}, f32[2,32,8,128]{3,2,1,0:T(8,128)}, u32[]{:S(2)}) copy-start(f32[2,32,8,128]{3,2,1,0:T(8,128)} %refs_11_.1) | copy-start | bytes 786436
  4.7 0.9 %copy-start.4 = (f32[2,8,16,128]{3,2,1,0:T(8,128)S(1)}, f32[2,8,16,128]{3,2,1,0:T(8,128)}, u32[]{:S(2)}) copy-start(f32[2,8,16,128]{3,2,1,0:T(8,128)} %refs_6_.1) | copy-start | bytes 393220
  5.6 0.9 %copy-start.5 = (f32[2,8,16,128]{3,2,1,0:T(8,128)S(1)}, f32[2,8,16,128]{3,2,1,0:T(8,128)}, u32[]{:S(2)}) copy-start(f32[2,8,16,128]{3,2,1,0:T(8,128)} %refs_7_.1) | copy-start | bytes 393220
  6.5 0.8 %copy-start.6 = (bf16[16,1024]{1,0:T(8,128)(2,1)S(1)}, bf16[16,1024]{1,0:T(8,128)(2,1)}, u32[]{:S(2)}) copy-start(bf16[16,1024]{1,0:T(8,128)(2,1)} %refs_0_.1) | copy-start | bytes 98308
  7.3 0.7 copy-start.7
  8.0 0.7 copy-start.8
  8.7 0.7 copy-start.9
  9.4 0.7 copy-start.10
  10.1 0.7 copy-start.11

commit v2 on v1

v2 whole, which is shorter than its diff:
```python
import functools

import jax
import jax.numpy as jnp
from jax import lax
from jax.experimental import pallas as pl
from jax.experimental.pallas import tpu as pltpu
from jax.sharding import PartitionSpec as P

epsilon = 1e-06
HIGHEST = lax.Precision.HIGHEST
NT = (((1,), (1,)), ((), ()))


def iota(shape, axis):
    return lax.broadcasted_iota(jnp.int32, shape, axis)


def kernel(n_tp, n_dp, width, *refs):
    (tok, gain, win, rate, freq, step, sin, rout, skip, vw, gw, st), refs = refs[:12], refs[12:]
    (out_tok, out_st), refs = refs[:2], refs[2:]
    (tok_v, gain_v, win_v, rate_v, freq_v, step_v, sin_v, rout_v, skip_v, out_w, st_v), refs = (
        refs[:11], refs[11:])
    (xg, sq_s, sq_r, part_s, part_r, ready, prod_s, prod_r, fin_s, fin_r,
     keep_v, base_v, lift_v, mix_v, new_v,
     load_sem, out_sem, x_sem, sq_sem, part_sem, ready_sem, prod_sem, weight_sem, fin_sem) = refs
    layers, rows, groups, entries = st_v.shape
    chans = part_s.shape[-1]
    per = chans // groups
    batch = n_dp * rows
    own, half = tok_v.shape
    n_q, n_e = n_tp // 2, 2 * n_dp
    t = lax.axis_index("tp")
    d = lax.axis_index("dp")
    q, y = t // 2, lax.rem(t, 2)
    e = y * n_dp + d
    twin = 1 - y
    mine = pl.ds(pl.multiple_of(y * half, half), half)
    other = pl.ds(pl.multiple_of(twin * half, half), half)

    pairs = [
        (tok.at[:, mine], xg.at[0, t]), (tok.at[:, other], tok_v),
        (rate, rate_v), (freq, freq_v), (step, step_v), (sin, sin_v), (rout, rout_v),
        (skip, skip_v), (st, st_v), (gain.at[:, mine], gain_v)]
    for layer in range(layers):
        pairs.append((win.at[layer, mine, :], win_v.at[layer, y]))
    for layer in range(layers):
        pairs.append((vw.at[layer, :, mine], out_w.at[layer, 0, y]))
        pairs.append((gw.at[layer, :, mine], out_w.at[layer, 1, y]))
    loads = [pltpu.make_async_copy(src, dst, load_sem.at[i]) for i, (src, dst) in enumerate(pairs)]
    for load in loads:
        load.start()

    barrier = pltpu.get_barrier_semaphore()

    def greet(tp, dp):
        pl.semaphore_signal(barrier, inc=1, device_id={"tp": tp, "dp": dp},
                            device_id_type=pl.DeviceIdType.MESH)

    for k in range(1, n_tp):
        greet(lax.rem(t + k, n_tp), d)
    for k in range(1, n_dp):
        greet(t, lax.rem(d + k, n_dp))
        greet(q * 2 + twin, lax.rem(d + k, n_dp))

    pending = []

    def send(tp, dp, src, dst, sems, index):
        copy = pltpu.make_async_remote_copy(
            src_ref=src, dst_ref=dst,
            send_sem=sems.at[(0,) + index], recv_sem=sems.at[(1,) + index],
            device_id={"tp": tp, "dp": dp}, device_id_type=pl.DeviceIdType.MESH)
        copy.start()
        pending.append(copy)
        return copy

    def send_twin(src, dst, sems, index):
        return send(q * 2 + twin, d, src, dst, sems, index)

    def send_group(pick, dst, sems, layer):
        copies = []
        for k in range(1, n_e):
            to = lax.rem(e + k, n_e)
            copies.append(send(q * 2 + to // n_dp, lax.rem(to, n_dp), pick(to), dst, sems,
                               (layer, k)))
        return copies

    def send_input(layer):
        return send_twin(win.at[layer, other, :], win_v.at[layer, y], weight_sem, (layer, 0))

    def send_output(layer, which):
        return send_twin((vw, gw)[which].at[layer, :, other], out_w.at[layer, which, y],
                         weight_sem, (layer, 1 + which))

    def prepare(layer):
        half = entries // 2
        diagonal = iota((groups, groups), 0) == iota((groups, groups), 1)
        step = jnp.sum(jnp.where(diagonal, step_v[layer][None, :], 0.0), axis=1, keepdims=True)
        rate = jnp.concatenate([rate_v[layer]] * 2, axis=1)
        freq = jnp.concatenate([freq_v[layer]] * 2, axis=1)
        sign = jnp.where(iota((groups, entries), 1) < half, -1.0, 1.0)
        magnitude = jnp.exp(-rate * step)
        angle = freq * step
        keep_real = magnitude * jnp.cos(angle)
        keep_imag = magnitude * jnp.sin(angle)
        minus_one = keep_real - 1.0
        denominator = rate * rate + freq * freq
        lift_real = (-minus_one * rate + keep_imag * freq) / denominator
        lift_imag = sign * (-keep_imag * rate - minus_one * freq) / denominator
        keep_imag = sign * keep_imag

        def swap(value):
            return jnp.concatenate([value[..., half:], value[..., :half]], axis=-1)

        matrix = sin_v[layer]
        lifted = lift_real[:, None, :] * matrix + lift_imag[:, None, :] * swap(matrix)
        lifted = lifted.reshape(chans, entries)
        read = rout_v[layer].reshape(chans, entries)
        mixed = lax.dot_general(lifted, read, NT, precision=HIGHEST,
                                preferred_element_type=jnp.float32)
        first, second = iota((chans, chans), 0), iota((chans, chans), 1)
        mixed = jnp.where(first // per == second // per, mixed, 0.0)
        mixed = mixed + jnp.where(first == second, skip_v[layer][None, :], 0.0)
        old = st_v[layer]
        kept = keep_real[None] * old + keep_imag[None] * swap(old)
        base = lax.dot_general(kept.reshape(rows * groups, entries), read, NT, precision=HIGHEST,
                               preferred_element_type=jnp.float32).reshape(rows, groups, chans)
        own = iota((groups, chans), 0) == iota((groups, chans), 1) // per
        keep_v[layer] = kept
        base_v[layer] = jnp.sum(jnp.where(own[None], base, 0.0), axis=1)
        lift_v[layer] = lifted
        mix_v[layer] = mixed

    loads[0].wait()
    loads[1].wait()
    pl.semaphore_wait(barrier, n_tp - 1 + 2 * (n_dp - 1))
    sent = []
    for k in range(1, n_q):
        to = lax.rem(q + k, n_q)
        sent.append(send(to * 2 + y, d, xg.at[0, t], xg.at[0, t], x_sem, (0, 0, k)))
        sent.append(send(to * 2 + twin, d, tok_v, xg.at[0, t], x_sem, (0, 1, k)))
    sent.append(send_twin(tok_v, xg.at[0, t], x_sem, (0, 1, 0)))
    inputs = [send_input(0)]
    outputs = [[send_output(0, 0)]]
    for load in loads[2:9]:
        load.wait()
    prepare(0)
    for load in loads[9:]:
        load.wait()
    outs = []

    for layer in range(layers):
        for copy in sent:
            copy.wait_recv()
        x = xg[layer].reshape(batch, half).astype(jnp.float32)
        square = jnp.sum(x * x, axis=1, keepdims=True)
        eye = iota((batch, batch), 0) == iota((batch, batch), 1)
        line = jnp.sum(jnp.where(eye, square, 0.0), axis=0, keepdims=True)
        sq_s[layer] = jnp.broadcast_to(line, (8, batch))
        sent = send_group(lambda to: sq_s.at[layer], sq_r.at[layer, e], sq_sem, layer)
        gained = (x * gain_v[layer][None, :]).astype(jnp.bfloat16)
        inputs[layer].wait_recv()
        for i in range(2):
            part = jnp.dot(gained, win_v[layer, i], preferred_element_type=jnp.float32)
            part_s[layer, pl.ds(i * n_dp, n_dp)] = part.reshape(n_dp, rows, chans)
        sent += send_group(lambda to: part_s.at[layer, to], part_r.at[layer, e], part_sem, layer)
        if layer == 0:
            outputs[0].append(send_output(0, 1))
        total = part_s[layer, e]
        for copy in sent:
            copy.wait_recv()
        for k in range(1, n_e):
            source = lax.rem(e + n_e - k, n_e)
            total += part_r[layer, source]
            line += sq_r[layer, source][:1]
        pick = iota((rows, batch), 1) == iota((rows, batch), 0) + d * rows
        square = jnp.sum(jnp.where(pick, line, 0.0), axis=1, keepdims=True)
        drive = total * lax.rsqrt(square / width + epsilon)
        value = base_v[layer] + jnp.dot(drive, mix_v[layer], precision=HIGHEST,
                                        preferred_element_type=jnp.float32)
        ready[layer, e] = jax.nn.gelu(value).astype(jnp.bfloat16)
        sent = send_group(lambda to: ready.at[layer, e], ready.at[layer, e], ready_sem, layer)
        mask = iota((groups, chans), 0) == iota((groups, chans), 1) // per
        spread = jnp.where(mask[None], drive[:, None, :], 0.0).reshape(rows * groups, chans)
        push = jnp.dot(spread, lift_v[layer], precision=HIGHEST, preferred_element_type=jnp.float32)
        new_v[layer] = keep_v[layer] + push.reshape(rows, groups, entries)
        out = pltpu.make_async_copy(new_v.at[layer], out_st.at[layer], out_sem.at[layer])
        out.start()
        outs.append(out)
        for copy in outputs[layer] + sent:
            copy.wait_recv()
        first = ready[layer, pl.ds(0, n_dp)].reshape(batch, chans)
        second = ready[layer, pl.ds(n_dp, n_dp)].reshape(batch, chans)
        every = jnp.concatenate([first, second], axis=1)
        sent = []
        for i in range(2):
            product = jnp.dot(every, out_w[layer, i].reshape(2 * chans, half),
                              preferred_element_type=jnp.float32)
            prod_s[layer, i] = product.astype(jnp.bfloat16).reshape(n_q, 2 * own, half)
            for k in range(1, n_q):
                to = lax.rem(q + k, n_q)
                sent.append(send(to * 2 + y, d, prod_s.at[layer, i, to], prod_r.at[layer, i, q],
                                 prod_sem, (layer, i, k)))
        if layer + 1 < layers:
            inputs.append(send_input(layer + 1))
            outputs.append([send_output(layer + 1, 0), send_output(layer + 1, 1)])
            prepare(layer + 1)
        for copy in sent:
            copy.wait_recv()
        both = []
        for i in range(2):
            total = prod_s[layer, i, q].astype(jnp.float32)
            for k in range(1, n_q):
                total += prod_r[layer, i, lax.rem(q + n_q - k, n_q)].astype(jnp.float32)
            both.append(total)
        block = pl.ds(2 * q, 2)
        current = xg[layer, block].reshape(2 * own, half).astype(jnp.float32)
        current = (current + both[0] * jax.nn.sigmoid(both[1])).astype(jnp.bfloat16)
        current = current.reshape(2, own, half)
        if layer + 1 < layers:
            xg[layer + 1, block] = current
            sent = []
            for k in range(1, n_q):
                sent.append(send(lax.rem(q + k, n_q) * 2 + y, d, xg.at[layer + 1, block],
                                 xg.at[layer + 1, block], x_sem, (layer + 1, 0, k)))
        else:
            fin_s[...] = current
            copy = send_twin(fin_s.at[twin], fin_r, fin_sem, ())
            here = fin_s[y]
            copy.wait_recv()
            there = fin_r[...]
            out_tok[:, :half] = jnp.where(y == 0, here, there)
            out_tok[:, half:] = jnp.where(y == 0, there, here)
    for out in outs:
        out.wait()
    for copy in pending:
        copy.wait_send()


def body(n_tp, n_dp, *args):
    tokens, states, win = args[0], args[11], args[2]
    layers, rows, groups, entries = states.shape
    local, chans = tokens.shape[1], win.shape[2]
    own, batch, half = tokens.shape[0], rows * n_dp, local // 2
    n_q, n_e = n_tp // 2, 2 * n_dp
    f32, bf16 = jnp.float32, jnp.bfloat16
    dma = pltpu.SemaphoreType.DMA
    any_spec = pl.BlockSpec(memory_space=pl.ANY)
    scratch = [
        pltpu.VMEM((own, half), bf16),
        pltpu.VMEM((layers, half), f32),
        pltpu.VMEM((layers, 2, half, chans), bf16),
        *[pltpu.VMEM(a.shape, a.dtype) for a in args[3:9]],
        pltpu.VMEM((layers, 2, 2, chans, half), bf16),
        pltpu.VMEM(states.shape, f32),
        pltpu.VMEM((layers, n_tp, own, half), bf16),
        pltpu.VMEM((layers, 8, batch), f32),
        pltpu.VMEM((layers, n_e, 8, batch), f32),
        pltpu.VMEM((layers, n_e, rows, chans), f32),
        pltpu.VMEM((layers, n_e, rows, chans), f32),
        pltpu.VMEM((layers, n_e, rows, chans), bf16),
        pltpu.VMEM((layers, 2, n_q, 2 * own, half), bf16),
        pltpu.VMEM((layers, 2, n_q, 2 * own, half), bf16),
        pltpu.VMEM((2, own, half), bf16),
        pltpu.VMEM((own, half), bf16),
        pltpu.VMEM(states.shape, f32),
        pltpu.VMEM((layers, rows, chans), f32),
        pltpu.VMEM((layers, chans, entries), f32),
        pltpu.VMEM((layers, chans, chans), f32),
        pltpu.VMEM(states.shape, f32),
        dma((10 + 3 * layers,)), dma((layers,)), dma((2, layers, 2, n_q)), dma((2, layers, n_e)),
        dma((2, layers, n_e)), dma((2, layers, n_e)), dma((2, layers, 2, n_q)),
        dma((2, layers, 3)), dma((2,)),
    ]
    return pl.pallas_call(
        functools.partial(kernel, n_tp, n_dp, float(local * n_dp)),
        out_shape=(jax.ShapeDtypeStruct(tokens.shape, bf16),
                   jax.ShapeDtypeStruct(states.shape, f32)),
        in_specs=[any_spec] * 12,
        out_specs=(pl.BlockSpec(memory_space=pltpu.VMEM), any_spec),
        scratch_shapes=scratch,
        compiler_params=pltpu.CompilerParams(
            collective_id=0, has_side_effects=True, vmem_limit_bytes=67043328),
    )(*args)


def solution(mesh):
    in_specs = (
        P("tp", "dp"),
        P(None, "dp"),
        P(None, "dp", "tp"),
        P(None, "tp", None),
        P(None, "tp", None),
        P(None, "tp"),
        P(None, "tp", None, None),
        P(None, "tp", None, None),
        P(None, "tp"),
        P(None, "tp", "dp"),
        P(None, "tp", "dp"),
        P(None, "dp", "tp", None),
    )
    out_specs = (P("tp", "dp"), P(None, "dp", "tp", None))
    run = functools.partial(body, mesh.shape["tp"], mesh.shape["dp"])
    return jax.shard_map(run, mesh=mesh, in_specs=in_specs, out_specs=out_specs, check_vma=False)
```

time: 72.5 us -> 56.4 us (0.78)
  local copies, waits for them, and re-layouts: 11.4 us -> 3.04 us
  Pallas kernels: 59.8 us -> 52.5 us
    unnamed x26 -> x2, local copies, waits for them, and re-layouts: 11.4 us -> 3.04 us
    pallas_call x1, Pallas kernels: 59.8 us -> 52.5 us  [body(): pl.pallas_call(functools.partial(kernel, n_tp, n_dp, float(local * n_dp))...]
where the time goes in v2:
time: 56.4 us; the launch traced here: 56.2 us
  Pallas kernels  52.5 us (93%)
  local copies, waits for them, and re-layouts  3.04 us (5%)
  between operations  0.64 us (1%)
    pallas_call x1, Pallas kernels, body(): pl.pallas_call(functools.partial(kernel, n_tp, n_dp, float(local * n_dp))...  52.5 us
    unnamed x2, local copies, waits for them, and re-layouts  3.04 us

profile of v2, /device:TPU:0, one launch (start us, length us, event | category | flops | bytes accessed | tf_op | source)
XLA Modules:
  0.0 56.2 jit_solution(3679383917093232399)
XLA Ops:
  0.6 52.5 %shard_map.131 = (bf16[16,1024]{1,0:T(8,128)(2,1)}, f32[2,32,8,128]{3,2,1,0:T(8,128)}) custom-call(bf16[16,1024]{1,0:T(8,128)(2,1)} %refs_0_.1, f32[2,1024]{1,0:T(2,128)} %refs_1_.1, bf16[2,1024,128]{2,1,0:T(8,128)(2,1)} %refs_2_.1, f32[2,8,64]{2,1,0:T(8,128)} %refs_3_.1, f32[2,8,64]{2,1,0:T(8,128)} %refs_4_.1, f32[2,8]{1,0:T(2,128)} %refs_5_.1, ...), custom_call_target="tpu_custom_call" | custom-call | tf_op jit(solution)/shard_map/pallas_call | solution.py:275
  53.1 1.4 %copy.16 = bf16[16,1024]{1,0:T(8,128)(2,1)} copy(bf16[16,1024]{1,0:T(8,128)(2,1)} %get-tuple-element.4) | data formatting | bytes 65536
  54.5 1.7 %copy.17 = f32[2,32,8,128]{3,2,1,0:T(8,128)} copy(f32[2,32,8,128]{3,2,1,0:T(8,128)} %get-tuple-element.5) | data formatting | bytes 524288

commit v3 on v2

--- a/solution.py
+++ b/solution.py
@@ -21,7 +21,7 @@
     (out_tok, out_st), refs = refs[:2], refs[2:]
     (tok_v, gain_v, win_v, rate_v, freq_v, step_v, sin_v, rout_v, skip_v, out_w, st_v), refs = (
         refs[:11], refs[11:])
-    (xg, sq_s, sq_r, part_s, part_r, ready, prod_s, prod_r, fin_s, fin_r,
+    (xg, sq_s, sq_r, part_v, part_s, part_r, ready, prod_s, prod_r, fin_s, fin_r,
      keep_v, base_v, lift_v, mix_v, new_v,
      load_sem, out_sem, x_sem, sq_sem, part_sem, ready_sem, prod_sem, weight_sem, fin_sem) = refs
     layers, rows, groups, entries = st_v.shape
@@ -63,6 +63,15 @@
         greet(t, lax.rem(d + k, n_dp))
         greet(q * 2 + twin, lax.rem(d + k, n_dp))
 
+    def partner(k):
+        to, bit = q, 1
+        while bit <= k:
+            if k & bit:
+                to = to + bit * (1 - 2 * lax.rem(q // bit, 2))
+            bit *= 2
+        return to
+
+    hops = range(n_q - 1, 0, -1)
     pending = []
 
     def send(tp, dp, src, dst, sems, index):
@@ -84,6 +93,11 @@
             copies.append(send(q * 2 + to // n_dp, lax.rem(to, n_dp), pick(to), dst, sems,
                                (layer, k)))
         return copies
+
+    def send_product(layer, i, k):
+        to = partner(k)
+        return send(to * 2 + y, d, prod_s.at[layer, i, to], prod_r.at[layer, i, q],
+                    prod_sem, (layer, i, k))
 
     def send_input(layer):
         return send_twin(win.at[layer, other, :], win_v.at[layer, y], weight_sem, (layer, 0))
@@ -135,8 +149,8 @@
     loads[1].wait()
     pl.semaphore_wait(barrier, n_tp - 1 + 2 * (n_dp - 1))
     sent = []
-    for k in range(1, n_q):
-        to = lax.rem(q + k, n_q)
+    for k in hops:
+        to = partner(k)
         sent.append(send(to * 2 + y, d, xg.at[0, t], xg.at[0, t], x_sem, (0, 0, k)))
         sent.append(send(to * 2 + twin, d, tok_v, xg.at[0, t], x_sem, (0, 1, k)))
     sent.append(send_twin(tok_v, xg.at[0, t], x_sem, (0, 1, 0)))
@@ -162,16 +176,18 @@
         inputs[layer].wait_recv()
         for i in range(2):
             part = jnp.dot(gained, win_v[layer, i], preferred_element_type=jnp.float32)
-            part_s[layer, pl.ds(i * n_dp, n_dp)] = part.reshape(n_dp, rows, chans)
+            part_v[layer, pl.ds(i * n_dp, n_dp)] = part.reshape(n_dp, rows, chans)
+            part_s[layer, pl.ds(i * n_dp, n_dp)] = (
+                part.astype(jnp.bfloat16).reshape(n_dp, rows, chans))
         sent += send_group(lambda to: part_s.at[layer, to], part_r.at[layer, e], part_sem, layer)
         if layer == 0:
             outputs[0].append(send_output(0, 1))
-        total = part_s[layer, e]
+        total = part_v[layer, e]
         for copy in sent:
             copy.wait_recv()
         for k in range(1, n_e):
             source = lax.rem(e + n_e - k, n_e)
-            total += part_r[layer, source]
+            total += part_r[layer, source].astype(jnp.float32)
             line += sq_r[layer, source][:1]
         pick = iota((rows, batch), 1) == iota((rows, batch), 0) + d * rows
         square = jnp.sum(jnp.where(pick, line, 0.0), axis=1, keepdims=True)
@@ -197,10 +213,8 @@
             product = jnp.dot(every, out_w[layer, i].reshape(2 * chans, half),
                               preferred_element_type=jnp.float32)
             prod_s[layer, i] = product.astype(jnp.bfloat16).reshape(n_q, 2 * own, half)
-            for k in range(1, n_q):
-                to = lax.rem(q + k, n_q)
-                sent.append(send(to * 2 + y, d, prod_s.at[layer, i, to], prod_r.at[layer, i, q],
-                                 prod_sem, (layer, i, k)))
+            sent += [send_product(layer, i, k) for k in hops if k > 1]
+        sent += [send_product(layer, i, 1) for i in range(2)]
         if layer + 1 < layers:
             inputs.append(send_input(layer + 1))
             outputs.append([send_output(layer + 1, 0), send_output(layer + 1, 1)])
@@ -211,7 +225,7 @@
         for i in range(2):
             total = prod_s[layer, i, q].astype(jnp.float32)
             for k in range(1, n_q):
-                total += prod_r[layer, i, lax.rem(q + n_q - k, n_q)].astype(jnp.float32)
+                total += prod_r[layer, i, partner(k)].astype(jnp.float32)
             both.append(total)
         block = pl.ds(2 * q, 2)
         current = xg[layer, block].reshape(2 * own, half).astype(jnp.float32)
@@ -220,8 +234,8 @@
         if layer + 1 < layers:
             xg[layer + 1, block] = current
             sent = []
-            for k in range(1, n_q):
-                sent.append(send(lax.rem(q + k, n_q) * 2 + y, d, xg.at[layer + 1, block],
+            for k in hops:
+                sent.append(send(partner(k) * 2 + y, d, xg.at[layer + 1, block],
                                  xg.at[layer + 1, block], x_sem, (layer + 1, 0, k)))
         else:
             fin_s[...] = current
@@ -257,7 +271,8 @@
         pltpu.VMEM((layers, 8, batch), f32),
         pltpu.VMEM((layers, n_e, 8, batch), f32),
         pltpu.VMEM((layers, n_e, rows, chans), f32),
-        pltpu.VMEM((layers, n_e, rows, chans), f32),
+        pltpu.VMEM((layers, n_e, rows, chans), bf16),
+        pltpu.VMEM((layers, n_e, rows, chans), bf16),
         pltpu.VMEM((layers, n_e, rows, chans), bf16),
         pltpu.VMEM((layers, 2, n_q, 2 * own, half), bf16),
         pltpu.VMEM((layers, 2, n_q, 2 * own, half), bf16),

time: 56.4 us -> 56.1 us (level)
  no operation moved by 1% of the time
where the time goes in v3:
time: 56.1 us; the launch traced here: 55.9 us
  Pallas kernels  52.2 us (93%)
  local copies, waits for them, and re-layouts  3.04 us (5%)
  between operations  0.64 us (1%)
    pallas_call x1, Pallas kernels, body(): pl.pallas_call(functools.partial(kernel, n_tp, n_dp, float(local * n_dp))...  52.2 us
    unnamed x2, local copies, waits for them, and re-layouts  3.04 us

profile of v3, /device:TPU:0, one launch (start us, length us, event | category | flops | bytes accessed | tf_op | source)
XLA Modules:
  0.0 55.9 jit_solution(13272378619089538164)
XLA Ops:
  0.6 52.2 %shard_map.131 = (bf16[16,1024]{1,0:T(8,128)(2,1)}, f32[2,32,8,128]{3,2,1,0:T(8,128)}) custom-call(bf16[16,1024]{1,0:T(8,128)(2,1)} %refs_0_.1, f32[2,1024]{1,0:T(2,128)} %refs_1_.1, bf16[2,1024,128]{2,1,0:T(8,128)(2,1)} %refs_2_.1, f32[2,8,64]{2,1,0:T(8,128)} %refs_3_.1, f32[2,8,64]{2,1,0:T(8,128)} %refs_4_.1, f32[2,8]{1,0:T(2,128)} %refs_5_.1, ...), custom_call_target="tpu_custom_call" | custom-call | tf_op jit(solution)/shard_map/pallas_call | solution.py:290
  52.8 1.4 %copy.16 = bf16[16,1024]{1,0:T(8,128)(2,1)} copy(bf16[16,1024]{1,0:T(8,128)(2,1)} %get-tuple-element.4) | data formatting | bytes 65536
  54.2 1.7 %copy.17 = f32[2,32,8,128]{3,2,1,0:T(8,128)} copy(f32[2,32,8,128]{3,2,1,0:T(8,128)} %get-tuple-element.5) | data formatting | bytes 524288

commit v4 on v3

--- a/solution.py
+++ b/solution.py
@@ -21,9 +21,9 @@
     (out_tok, out_st), refs = refs[:2], refs[2:]
     (tok_v, gain_v, win_v, rate_v, freq_v, step_v, sin_v, rout_v, skip_v, out_w, st_v), refs = (
         refs[:11], refs[11:])
-    (xg, sq_s, sq_r, part_v, part_s, part_r, ready, prod_s, prod_r, fin_s, fin_r,
+    (xg, sq_s, sq_r, part_v, part_s, part_r, ready, prod_s, prod_r, last_r, fin_r,
      keep_v, base_v, lift_v, mix_v, new_v,
-     load_sem, out_sem, x_sem, sq_sem, part_sem, ready_sem, prod_sem, weight_sem, fin_sem) = refs
+     load_sem, out_sem, x_sem, sq_sem, part_sem, ready_sem, prod_sem, weight_sem, fin_sem, last_sem) = refs
     layers, rows, groups, entries = st_v.shape
     chans = part_s.shape[-1]
     per = chans // groups
@@ -98,6 +98,12 @@
         to = partner(k)
         return send(to * 2 + y, d, prod_s.at[layer, i, to], prod_r.at[layer, i, q],
                     prod_sem, (layer, i, k))
+
+    def send_last(i, cross, k):
+        row = twin if cross else y
+        to = partner(k)
+        return send(to * 2 + row, d, prod_s.at[layers - 1, i, to, row], last_r.at[i, t],
+                    last_sem, (i, cross, k))
 
     def send_input(layer):
         return send_twin(win.at[layer, other, :], win_v.at[layer, y], weight_sem, (layer, 0))
@@ -212,39 +218,54 @@
         for i in range(2):
             product = jnp.dot(every, out_w[layer, i].reshape(2 * chans, half),
                               preferred_element_type=jnp.float32)
-            prod_s[layer, i] = product.astype(jnp.bfloat16).reshape(n_q, 2 * own, half)
-            sent += [send_product(layer, i, k) for k in hops if k > 1]
-        sent += [send_product(layer, i, 1) for i in range(2)]
+            prod_s[layer, i] = product.astype(jnp.bfloat16).reshape(n_q, 2, own, half)
+            if layer + 1 < layers:
+                sent += [send_product(layer, i, k) for k in hops if k > 1]
+            else:
+                sent += [send_last(i, c, k) for k in hops if k > 1 for c in (1, 0)]
+        if layer + 1 < layers:
+            sent += [send_product(layer, i, 1) for i in range(2)]
+        else:
+            sent += [send_last(i, c, k) for c, k in ((1, 1), (0, 1), (1, 0)) for i in range(2)]
         if layer + 1 < layers:
             inputs.append(send_input(layer + 1))
             outputs.append([send_output(layer + 1, 0), send_output(layer + 1, 1)])
             prepare(layer + 1)
         for copy in sent:
             copy.wait_recv()
-        both = []
-        for i in range(2):
-            total = prod_s[layer, i, q].astype(jnp.float32)
-            for k in range(1, n_q):
-                total += prod_r[layer, i, partner(k)].astype(jnp.float32)
-            both.append(total)
-        block = pl.ds(2 * q, 2)
-        current = xg[layer, block].reshape(2 * own, half).astype(jnp.float32)
-        current = (current + both[0] * jax.nn.sigmoid(both[1])).astype(jnp.bfloat16)
-        current = current.reshape(2, own, half)
+        f32 = jnp.float32
         if layer + 1 < layers:
-            xg[layer + 1, block] = current
+            both = []
+            for i in range(2):
+                total = prod_s[layer, i, q].astype(f32)
+                for k in range(1, n_q):
+                    total += prod_r[layer, i, partner(k)].astype(f32)
+                both.append(total)
+            block = pl.ds(2 * q, 2)
+            current = xg[layer, block].astype(f32) + both[0] * jax.nn.sigmoid(both[1])
+            xg[layer + 1, block] = current.astype(jnp.bfloat16)
             sent = []
             for k in hops:
                 sent.append(send(partner(k) * 2 + y, d, xg.at[layer + 1, block],
                                  xg.at[layer + 1, block], x_sem, (layer + 1, 0, k)))
+            if layer + 2 == layers:
+                rest = send_twin(xg.at[layer + 1, q * 2 + twin], fin_r, fin_sem, ())
         else:
-            fin_s[...] = current
-            copy = send_twin(fin_s.at[twin], fin_r, fin_sem, ())
-            here = fin_s[y]
-            copy.wait_recv()
-            there = fin_r[...]
-            out_tok[:, :half] = jnp.where(y == 0, here, there)
-            out_tok[:, half:] = jnp.where(y == 0, there, here)
+            rest.wait_recv()
+            same, cross = [], []
+            for i in range(2):
+                total = prod_s[layer, i, q, y].astype(f32)
+                for k in range(1, n_q):
+                    total += last_r[i, partner(k) * 2 + y].astype(f32)
+                same.append(total)
+                total = last_r[i, q * 2 + twin].astype(f32)
+                for k in range(1, n_q):
+                    total += last_r[i, partner(k) * 2 + twin].astype(f32)
+                cross.append(total)
+            here = xg[layer, t].astype(f32) + same[0] * jax.nn.sigmoid(same[1])
+            there = fin_r[...].astype(f32) + cross[0] * jax.nn.sigmoid(cross[1])
+            out_tok[:, :half] = jnp.where(y == 0, here, there).astype(jnp.bfloat16)
+            out_tok[:, half:] = jnp.where(y == 0, there, here).astype(jnp.bfloat16)
     for out in outs:
         out.wait()
     for copy in pending:
@@ -274,9 +295,9 @@
         pltpu.VMEM((layers, n_e, rows, chans), bf16),
         pltpu.VMEM((layers, n_e, rows, chans), bf16),
         pltpu.VMEM((layers, n_e, rows, chans), bf16),
-        pltpu.VMEM((layers, 2, n_q, 2 * own, half), bf16),
-        pltpu.VMEM((layers, 2, n_q, 2 * own, half), bf16),
-        pltpu.VMEM((2, own, half), bf16),
+        pltpu.VMEM((layers, 2, n_q, 2, own, half), bf16),
+        pltpu.VMEM((layers - 1, 2, n_q, 2, own, half), bf16),
+        pltpu.VMEM((2, n_tp, own, half), bf16),
         pltpu.VMEM((own, half), bf16),
         pltpu.VMEM(states.shape, f32),
         pltpu.VMEM((layers, rows, chans), f32),
@@ -285,7 +306,7 @@
         pltpu.VMEM(states.shape, f32),
         dma((10 + 3 * layers,)), dma((layers,)), dma((2, layers, 2, n_q)), dma((2, layers, n_e)),
         dma((2, layers, n_e)), dma((2, layers, n_e)), dma((2, layers, 2, n_q)),
-        dma((2, layers, 3)), dma((2,)),
+        dma((2, layers, 3)), dma((2,)), dma((2, 2, 2, n_q)),
     ]
     return pl.pallas_call(
         functools.partial(kernel, n_tp, n_dp, float(local * n_dp)),

time: 56.1 us -> 53.9 us (0.961)
  Pallas kernels: 52.2 us -> 50 us
    pallas_call x1, Pallas kernels: 52.2 us -> 50 us  [body(): pl.pallas_call(functools.partial(kernel, n_tp, n_dp, float(local * n_dp))...]
where the time goes in v4:
time: 53.9 us; the launch traced here: 53.7 us
  Pallas kernels  50 us (93%)
  local copies, waits for them, and re-layouts  3.04 us (6%)
  between operations  0.64 us (1%)
    pallas_call x1, Pallas kernels, body(): pl.pallas_call(functools.partial(kernel, n_tp, n_dp, float(local * n_dp))...  50 us
    unnamed x2, local copies, waits for them, and re-layouts  3.04 us

profile of v4, /device:TPU:0, one launch (start us, length us, event | category | flops | bytes accessed | tf_op | source)
XLA Modules:
  0.0 53.7 jit_solution(14685471469390006804)
XLA Ops:
  0.6 50.0 %shard_map.131 = (bf16[16,1024]{1,0:T(8,128)(2,1)}, f32[2,32,8,128]{3,2,1,0:T(8,128)}) custom-call(bf16[16,1024]{1,0:T(8,128)(2,1)} %refs_0_.1, f32[2,1024]{1,0:T(2,128)} %refs_1_.1, bf16[2,1024,128]{2,1,0:T(8,128)(2,1)} %refs_2_.1, f32[2,8,64]{2,1,0:T(8,128)} %refs_3_.1, f32[2,8,64]{2,1,0:T(8,128)} %refs_4_.1, f32[2,8]{1,0:T(2,128)} %refs_5_.1, ...), custom_call_target="tpu_custom_call" | custom-call | tf_op jit(solution)/shard_map/pallas_call | solution.py:311
  50.7 1.4 %copy.16 = bf16[16,1024]{1,0:T(8,128)(2,1)} copy(bf16[16,1024]{1,0:T(8,128)(2,1)} %get-tuple-element.4) | data formatting | bytes 65536
  52.0 1.7 %copy.17 = f32[2,32,8,128]{3,2,1,0:T(8,128)} copy(f32[2,32,8,128]{3,2,1,0:T(8,128)} %get-tuple-element.5) | data formatting | bytes 524288

commit v5 on v4

--- a/solution.py
+++ b/solution.py
@@ -21,9 +21,9 @@
     (out_tok, out_st), refs = refs[:2], refs[2:]
     (tok_v, gain_v, win_v, rate_v, freq_v, step_v, sin_v, rout_v, skip_v, out_w, st_v), refs = (
         refs[:11], refs[11:])
-    (xg, sq_s, sq_r, part_v, part_s, part_r, ready, prod_s, prod_r, last_r, fin_r,
+    (xg, sq_s, sq_r, part_v, part_s, part_r, ready, prod_s, prod_r, last_r, fin_r, relay_s, relay_r,
      keep_v, base_v, lift_v, mix_v, new_v,
-     load_sem, out_sem, x_sem, sq_sem, part_sem, ready_sem, prod_sem, weight_sem, fin_sem, last_sem) = refs
+     load_sem, out_sem, x_sem, sq_sem, part_sem, ready_sem, prod_sem, weight_sem, fin_sem, last_sem, relay_sem) = refs
     layers, rows, groups, entries = st_v.shape
     chans = part_s.shape[-1]
     per = chans // groups
@@ -94,9 +94,16 @@
                                (layer, k)))
         return copies
 
-    def send_product(layer, i, k):
+    far = range(n_q - 1, 1, -2)
+    heard = (1,) + tuple(k - 1 for k in far)
+
+    def send_relay(layer, i, k):
+        return send(partner(1) * 2 + y, d, prod_s.at[layer, i, partner(k)],
+                    relay_r.at[layer, i, k // 2], relay_sem, (layer, i, k // 2))
+
+    def send_product(layer, i, k, source):
         to = partner(k)
-        return send(to * 2 + y, d, prod_s.at[layer, i, to], prod_r.at[layer, i, q],
+        return send(to * 2 + y, d, source, prod_r.at[layer, i, q],
                     prod_sem, (layer, i, k))
 
     def send_last(i, cross, k):
@@ -214,17 +221,24 @@
         first = ready[layer, pl.ds(0, n_dp)].reshape(batch, chans)
         second = ready[layer, pl.ds(n_dp, n_dp)].reshape(batch, chans)
         every = jnp.concatenate([first, second], axis=1)
-        sent = []
+        sent, relays = [], []
         for i in range(2):
             product = jnp.dot(every, out_w[layer, i].reshape(2 * chans, half),
                               preferred_element_type=jnp.float32)
             prod_s[layer, i] = product.astype(jnp.bfloat16).reshape(n_q, 2, own, half)
             if layer + 1 < layers:
-                sent += [send_product(layer, i, k) for k in hops if k > 1]
+                relays.append([send_relay(layer, i, k) for k in far])
             else:
                 sent += [send_last(i, c, k) for k in hops if k > 1 for c in (1, 0)]
         if layer + 1 < layers:
-            sent += [send_product(layer, i, 1) for i in range(2)]
+            sent += [send_product(layer, i, 1, prod_s.at[layer, i, partner(1)]) for i in range(2)]
+            for i in range(2):
+                for copy, k in zip(relays[i], far):
+                    copy.wait_recv()
+                    joined = (prod_s[layer, i, partner(k - 1)].astype(jnp.float32)
+                              + relay_r[layer, i, k // 2].astype(jnp.float32))
+                    relay_s[layer, i, k // 2] = joined.astype(jnp.bfloat16)
+                    sent.append(send_product(layer, i, k - 1, relay_s.at[layer, i, k // 2]))
         else:
             sent += [send_last(i, c, k) for c, k in ((1, 1), (0, 1), (1, 0)) for i in range(2)]
         if layer + 1 < layers:
@@ -238,7 +252,7 @@
             both = []
             for i in range(2):
                 total = prod_s[layer, i, q].astype(f32)
-                for k in range(1, n_q):
+                for k in heard:
                     total += prod_r[layer, i, partner(k)].astype(f32)
                 both.append(total)
             block = pl.ds(2 * q, 2)
@@ -299,6 +313,7 @@
         pltpu.VMEM((layers - 1, 2, n_q, 2, own, half), bf16),
         pltpu.VMEM((2, n_tp, own, half), bf16),
         pltpu.VMEM((own, half), bf16),
+        *[pltpu.VMEM((layers - 1, 2, n_q // 2, 2, own, half), bf16)] * 2,
         pltpu.VMEM(states.shape, f32),
         pltpu.VMEM((layers, rows, chans), f32),
         pltpu.VMEM((layers, chans, entries), f32),
@@ -307,6 +322,7 @@
         dma((10 + 3 * layers,)), dma((layers,)), dma((2, layers, 2, n_q)), dma((2, layers, n_e)),
         dma((2, layers, n_e)), dma((2, layers, n_e)), dma((2, layers, 2, n_q)),
         dma((2, layers, 3)), dma((2,)), dma((2, 2, 2, n_q)),
+        dma((2, layers - 1, 2, n_q // 2)),
     ]
     return pl.pallas_call(
         functools.partial(kernel, n_tp, n_dp, float(local * n_dp)),

time: 53.9 us -> 53.8 us (level)
  no operation moved by 1% of the time
where the time goes in v5:
time: 53.8 us; the launch traced here: 53.6 us
  Pallas kernels  49.9 us (93%)
  local copies, waits for them, and re-layouts  3.04 us (6%)
  between operations  0.64 us (1%)
    pallas_call x1, Pallas kernels, body(): pl.pallas_call(functools.partial(kernel, n_tp, n_dp, float(local * n_dp))...  49.9 us
    unnamed x2, local copies, waits for them, and re-layouts  3.04 us

profile of v5, /device:TPU:0, one launch (start us, length us, event | category | flops | bytes accessed | tf_op | source)
XLA Modules:
  0.0 53.6 jit_solution(11250374516499223431)
XLA Ops:
  0.6 49.9 %shard_map.131 = (bf16[16,1024]{1,0:T(8,128)(2,1)}, f32[2,32,8,128]{3,2,1,0:T(8,128)}) custom-call(bf16[16,1024]{1,0:T(8,128)(2,1)} %refs_0_.1, f32[2,1024]{1,0:T(2,128)} %refs_1_.1, bf16[2,1024,128]{2,1,0:T(8,128)(2,1)} %refs_2_.1, f32[2,8,64]{2,1,0:T(8,128)} %refs_3_.1, f32[2,8,64]{2,1,0:T(8,128)} %refs_4_.1, f32[2,8]{1,0:T(2,128)} %refs_5_.1, ...), custom_call_target="tpu_custom_call" | custom-call | tf_op jit(solution)/shard_map/pallas_call | solution.py:327
  50.5 1.4 %copy.16 = bf16[16,1024]{1,0:T(8,128)(2,1)} copy(bf16[16,1024]{1,0:T(8,128)(2,1)} %get-tuple-element.4) | data formatting | bytes 65536
  51.9 1.7 %copy.17 = f32[2,32,8,128]{3,2,1,0:T(8,128)} copy(f32[2,32,8,128]{3,2,1,0:T(8,128)} %get-tuple-element.5) | data formatting | bytes 524288

commit v6 on v5

--- a/solution.py
+++ b/solution.py
@@ -180,11 +180,6 @@
         for copy in sent:
             copy.wait_recv()
         x = xg[layer].reshape(batch, half).astype(jnp.float32)
-        square = jnp.sum(x * x, axis=1, keepdims=True)
-        eye = iota((batch, batch), 0) == iota((batch, batch), 1)
-        line = jnp.sum(jnp.where(eye, square, 0.0), axis=0, keepdims=True)
-        sq_s[layer] = jnp.broadcast_to(line, (8, batch))
-        sent = send_group(lambda to: sq_s.at[layer], sq_r.at[layer, e], sq_sem, layer)
         gained = (x * gain_v[layer][None, :]).astype(jnp.bfloat16)
         inputs[layer].wait_recv()
         for i in range(2):
@@ -192,7 +187,12 @@
             part_v[layer, pl.ds(i * n_dp, n_dp)] = part.reshape(n_dp, rows, chans)
             part_s[layer, pl.ds(i * n_dp, n_dp)] = (
                 part.astype(jnp.bfloat16).reshape(n_dp, rows, chans))
-        sent += send_group(lambda to: part_s.at[layer, to], part_r.at[layer, e], part_sem, layer)
+        sent = send_group(lambda to: part_s.at[layer, to], part_r.at[layer, e], part_sem, layer)
+        square = jnp.sum(x * x, axis=1, keepdims=True)
+        eye = iota((batch, batch), 0) == iota((batch, batch), 1)
+        line = jnp.sum(jnp.where(eye, square, 0.0), axis=0, keepdims=True)
+        sq_s[layer] = jnp.broadcast_to(line, (8, batch))
+        sent += send_group(lambda to: sq_s.at[layer], sq_r.at[layer, e], sq_sem, layer)
         if layer == 0:
             outputs[0].append(send_output(0, 1))
         total = part_v[layer, e]

time: 53.8 us -> 54 us (level)
  no operation moved by 1% of the time
where the time goes in v6:
time: 54 us; the launch traced here: 53.8 us
  Pallas kernels  50.1 us (93%)
  local copies, waits for them, and re-layouts  3.04 us (6%)
  between operations  0.64 us (1%)
    pallas_call x1, Pallas kernels, body(): pl.pallas_call(functools.partial(kernel, n_tp, n_dp, float(local * n_dp))...  50.1 us
    unnamed x2, local copies, waits for them, and re-layouts  3.04 us

profile of v6, /device:TPU:0, one launch (start us, length us, event | category | flops | bytes accessed | tf_op | source)
XLA Modules:
  0.0 53.8 jit_solution(4698818979939612101)
XLA Ops:
  0.6 50.1 %shard_map.131 = (bf16[16,1024]{1,0:T(8,128)(2,1)}, f32[2,32,8,128]{3,2,1,0:T(8,128)}) custom-call(bf16[16,1024]{1,0:T(8,128)(2,1)} %refs_0_.1, f32[2,1024]{1,0:T(2,128)} %refs_1_.1, bf16[2,1024,128]{2,1,0:T(8,128)(2,1)} %refs_2_.1, f32[2,8,64]{2,1,0:T(8,128)} %refs_3_.1, f32[2,8,64]{2,1,0:T(8,128)} %refs_4_.1, f32[2,8]{1,0:T(2,128)} %refs_5_.1, ...), custom_call_target="tpu_custom_call" | custom-call | tf_op jit(solution)/shard_map/pallas_call | solution.py:327
  50.7 1.4 %copy.16 = bf16[16,1024]{1,0:T(8,128)(2,1)} copy(bf16[16,1024]{1,0:T(8,128)(2,1)} %get-tuple-element.4) | data formatting | bytes 65536
  52.1 1.7 %copy.17 = f32[2,32,8,128]{3,2,1,0:T(8,128)} copy(f32[2,32,8,128]{3,2,1,0:T(8,128)} %get-tuple-element.5) | data formatting | bytes 524288
